TPU v7x, 32 devices: a whole 2x2x4 slice. The times are simulated.
32 devices in a mesh: rep: 2 (over y), fs: 4 (over z), tp: 4 (over x, core).
Axes of the slice: x: 2, y: 2, z: 4, core: 2. Of those that a mesh axis runs over, the one named last changes fastest.
Arguments:
- tokens: bfloat16 [2048, 2048], P(('rep', 'fs')), may hold values from -6 to 6
- gate_weight: bfloat16 [2048, 2816], P('fs', 'tp'), may hold values from -0.125 to 0.125
- up_weight: bfloat16 [2048, 2816], P('fs', 'tp'), may hold values from -0.125 to 0.125
- down_weight: bfloat16 [2816, 2048], P('tp', 'fs'), may hold values from -0.109375 to 0.109375
- out_grad: bfloat16 [2048, 2048], P(('rep', 'fs')), may hold values from -6 to 6
Outputs:
- input_grad: bfloat16 [2048, 2048], P(('rep', 'fs'))
- down_grad: float32 [2816, 2048], P('tp', 'fs')
- row_norms: float32 [2816], P('tp')
All inputs are finite; a program needn't handle non-finite values.
Results may differ from a plain program's by a relative error of at most 0.024.
Values may be sent and summed in bfloat16 or wider, within the bound.
A program may use at most 64 MiB of HBM per device.

v0:
```python
import jax
import jax.numpy as jnp
from jax import lax
from jax.sharding import PartitionSpec as P


def contract_last(left, right):
    return lax.dot_general(
        left, right, (((1,), (1,)), ((), ())), preferred_element_type=jnp.float32
    )


def contract_first(left, right):
    return lax.dot_general(
        left, right, (((0,), (0,)), ((), ())), preferred_element_type=jnp.float32
    )


def on_device(tokens, gate_weight, up_weight, down_weight, out_grad):
    down_full = lax.all_gather(down_weight, "fs", axis=1, tiled=True)
    gate_full, up_full = (
        lax.all_gather(gate_weight, "fs", axis=0, tiled=True),
        lax.all_gather(up_weight, "fs", axis=0, tiled=True),
    )
    gate_pre = jnp.dot(tokens, gate_full, preferred_element_type=jnp.float32)
    up_pre = jnp.dot(tokens, up_full, preferred_element_type=jnp.float32)
    sigma = jax.nn.sigmoid(gate_pre)
    activated = gate_pre * sigma
    hidden = (activated * up_pre).astype(jnp.bfloat16)
    hid_grad = contract_last(out_grad, down_full)
    up_grad = (hid_grad * activated).astype(jnp.bfloat16)
    gate_grad = (hid_grad * up_pre * sigma * (1.0 + gate_pre * (1.0 - sigma))).astype(jnp.bfloat16)
    partial_value = contract_last(gate_grad, gate_full) + contract_last(up_grad, up_full)
    input_grad = lax.psum(partial_value.astype(jnp.bfloat16), "tp")
    columns = lax.all_to_all(out_grad, "fs", split_axis=1, concat_axis=0, tiled=True)
    shard = contract_first(lax.all_gather(hidden, "fs", axis=0, tiled=True), columns)
    shard = lax.psum(shard.astype(jnp.bfloat16), "rep").astype(jnp.float32)
    norms = lax.psum(jnp.sum(shard * shard, axis=1), "fs")
    return (input_grad, shard, norms)


def solution(mesh):
    return jax.shard_map(
        on_device,
        mesh=mesh,
        in_specs=(
            P(("rep", "fs"), None),
            P("fs", "tp"),
            P("fs", "tp"),
            P("tp", "fs"),
            P(("rep", "fs"), None),
        ),
        out_specs=(P(("rep", "fs"), None), P("tp", "fs"), P("tp")),
        check_vma=False,
    )
```

profile of v0, /device:TPU:0, one launch (start us, length us, event | category | flops | bytes accessed | tf_op | source)
XLA Modules:
  0.0 329.1 jit_solution(854777100918134661)
XLA Ops:
  7.2 0.0 copy-start
  7.2 0.0 all-gather.9.cloned.1.call-start
  7.2 0.7 all-gather.9.cloned.1.call-update
  7.9 0.0 all-gather.7.cloned.1.call-start
  8.0 0.7 all-gather.7.cloned.1.call-update
  8.7 0.0 all-gather.5.cloned.1.call-start
  8.7 0.7 all-gather.5.cloned.1.call-update
  9.4 0.0 all-gather.11.cloned.1.call-start
  9.4 62.0 %all-gather.9.cloned.1.call-done = bf16[2048,704]{0,1:T(8,128)(2,1)} async-done(((bf16[512,704]{0,1:T(8,128)(2,1)}), bf16[2048,704]{0,1:T(8,128)(2,1)}) %all-gather.9.cloned.1.call-update) | async-done | bytes 2883600 | tf_op jit(solution)/shard_map/all_gather | solution.py:22
  71.4 0.0 copy-done
  71.4 2.8 fusion.8
  74.2 0.0 copy-start.3
  74.2 0.0 copy-start.2
  74.2 56.6 %all-gather.7.cloned.1.call-done = bf16[2048,704]{0,1:T(8,128)(2,1)} async-done(((bf16[512,704]{0,1:T(8,128)(2,1)}), bf16[2048,704]{0,1:T(8,128)(2,1)}) %all-gather.7.cloned.1.call-update) | async-done | bytes 2883600 | tf_op jit(solution)/shard_map/all_gather | solution.py:23
  130.8 3.7 %multiply_convert_fusion = (bf16[256,704]{0,1:T(8,128)(2,1)}, f32[256,704]{0,1:T(8,128)}) fusion(f32[256,704]{0,1:T(8,128)S(1)} %fusion.8, bf16[256,2048]{1,0:T(8,128)(2,1)S(1)} %copy-done, bf16[2048,704]{0,1:T(8,128)(2,1)} %all-gather.7.cloned.1.call-done), kind=kOutput, calls=%fused_computation.4 | convolution fusion | flops 739278848 | bytes 5734400 | tf_op jit(solution)/shard_map/dot_general | solution.py:26
  134.6 0.0 copy-done.3
  134.6 0.0 all-gather.11.cloned.1.call-update
  134.6 0.0 all-reduce.5.cloned.1.call-start
  134.6 0.0 copy-done.2
  134.7 0.5 copy.8
  135.2 56.6 %all_to_all.19 = bf16[256,4,512]{0,2,1:T(8,128)(2,1)S(1)} all-to-all(bf16[256,4,512]{0,2,1:T(8,128)(2,1)S(1)} %bitcast.14), channel_id=1, replica_groups=mesh['rep'=2,'fs'=4,'tp'=4] {'fs'}, dimensions={1} | all-to-all | bytes 2097152 | tf_op jit(solution)/shard_map/all_to_all | solution.py:35
  191.8 0.5 copy.9
  192.4 17.8 %all-gather.5.cloned.1.call-done = bf16[704,2048]{1,0:T(8,128)(2,1)} async-done(((bf16[704,512]{1,0:T(8,128)(2,1)}), bf16[704,2048]{1,0:T(8,128)(2,1)}) %all-gather.5.cloned.1.call-update) | async-done | bytes 2883600 | tf_op jit(solution)/shard_map/all_gather | solution.py:20
  210.1 3.9 %fusion.7 = f32[256,704]{0,1:T(8,128)} fusion(bf16[256,2048]{1,0:T(8,128)(2,1)} %param.9, bf16[704,2048]{1,0:T(8,128)(2,1)} %all-gather.5.cloned.1.call-done), kind=kOutput, calls=%fused_computation.13 | convolution fusion | flops 738197504 | bytes 4653056 | tf_op jit(solution)/shard_map/dot_general | solution.py:8
  214.1 32.2 %all-gather.11.cloned.1.call-done = bf16[1024,704]{0,1:T(8,128)(2,1)} async-done(((bf16[256,704]{0,1:T(8,128)(2,1)}), bf16[1024,704]{0,1:T(8,128)(2,1)}) %all-gather.11.cloned.1.call-update) | async-done | bytes 1441808 | tf_op jit(solution)/shard_map/all_gather | solution.py:36
  246.3 0.0 copy-start.4
  246.3 3.2 convolution_convert_fusion
  249.5 0.0 all-reduce.5.cloned.1.call-update
  249.5 0.0 all-reduce.3.cloned.1.call-start
  249.6 0.0 copy-done.4
  249.6 0.0 copy-start.1
  249.6 0.0 copy-start.5
  249.6 3.5 %fusion.2 = f32[256,2048]{1,0:T(8,128)S(1)} fusion(bf16[2048,704]{0,1:T(8,128)(2,1)} %all-gather.9.cloned.1.call-done, f32[256,704]{0,1:T(8,128)S(1)} %copy-done.4, f32[256,704]{0,1:T(8,128)} %fusion.7, f32[256,704]{0,1:T(8,128)} %get-tuple-element.6), kind=kOutput, calls=%fused_computation.9 | convolution fusion | flops 739999744 | bytes 7143424 | tf_op jit(solution)/shard_map/dot_general | solution.py:8
  253.1 0.0 copy-done.1
  253.1 0.0 copy-done.5
  253.1 2.0 fusion
  255.2 0.0 all-reduce.3.cloned.1.call-update
  255.2 25.6 %all-reduce.5.cloned.1.call-done = bf16[704,512]{1,0:T(8,128)(2,1)} async-done(((bf16[704,512]{1,0:T(8,128)(2,1)}), bf16[704,512]{1,0:T(8,128)(2,1)}) %all-reduce.5.cloned.1.call-update) | async-done | bytes 720912 | tf_op jit(solution)/shard_map/psum | solution.py:37
  280.8 2.3 multiply_reduce_fusion
  283.1 12.2 %psum.23 = f32[704]{0:T(1024)} all-reduce(f32[704]{0:T(1024)S(1)} %get-tuple-element.3), channel_id=1, replica_groups=mesh['rep'=2,'fs'=4,'tp'=4] {'fs'}, use_global_device_ids=true, to_apply=%region_3.0 | all-reduce | flops 704 | bytes 5632 | tf_op jit(solution)/shard_map/psum | solution.py:38
  295.4 24.5 %all-reduce.3.cloned.1.call-done = bf16[256,2048]{1,0:T(8,128)(2,1)} async-done(((bf16[256,2048]{1,0:T(8,128)(2,1)}), bf16[256,2048]{1,0:T(8,128)(2,1)}) %all-reduce.3.cloned.1.call-update) | async-done | bytes 1048592 | tf_op jit(solution)/shard_map/psum | solution.py:34
  319.9 2.3 copy.12
Async XLA Ops:
  7.2 64.3 %copy-start = (bf16[256,2048]{1,0:T(8,128)(2,1)S(1)}, bf16[256,2048]{1,0:T(8,128)(2,1)}, u32[]{:S(2)}) copy-start(bf16[256,2048]{1,0:T(8,128)(2,1)} %param.5) | copy-start | bytes 3145732
  7.2 64.2 %all-gather.9.cloned.1.call-start = ((), (), s32[]{:S(2)}) async-start(), calls=%async_computation.3 | async-start | bytes 3604480 | tf_op jit(solution)/shard_map/all_gather | solution.py:22
  7.9 122.9 %all-gather.7.cloned.1.call-start = ((), (), s32[]{:S(2)}) async-start(), calls=%async_computation.2 | async-start | bytes 3604480 | tf_op jit(solution)/shard_map/all_gather | solution.py:23
  8.7 201.5 %all-gather.5.cloned.1.call-start = ((), (), s32[]{:S(2)}) async-start(), calls=%async_computation.1 | async-start | bytes 3604480 | tf_op jit(solution)/shard_map/all_gather | solution.py:20
  9.4 236.9 %all-gather.11.cloned.1.call-start = ((), (), s32[]{:S(2)}) async-start(), calls=%async_computation.5 | async-start | bytes 1802240 | tf_op jit(solution)/shard_map/all_gather | solution.py:36
  74.2 60.4 %copy-start.3 = (f32[256,704]{0,1:T(8,128)}, f32[256,704]{0,1:T(8,128)S(1)}, u32[]{:S(2)}) copy-start(f32[256,704]{0,1:T(8,128)S(1)} %fusion.8) | copy-start | bytes 2162692
  74.2 60.4 %copy-start.2 = (bf16[256,2048]{1,0:T(8,128)(2,1)S(1)}, bf16[256,2048]{1,0:T(8,128)(2,1)}, u32[]{:S(2)}) copy-start(bf16[256,2048]{1,0:T(8,128)(2,1)} %param.9) | copy-start | bytes 3145732
  134.6 146.2 %all-reduce.5.cloned.1.call-start = ((), (), s32[]{:S(2)}) async-start(), calls=%async_computation.6 | async-start | bytes 1441792 | tf_op jit(solution)/shard_map/psum | solution.py:37
  246.3 3.3 %copy-start.4 = (f32[256,704]{0,1:T(8,128)S(1)}, f32[256,704]{0,1:T(8,128)}, u32[]{:S(2)}) copy-start(f32[256,704]{0,1:T(8,128)} %copy-done.3) | copy-start | bytes 2162692
  249.5 70.4 %all-reduce.3.cloned.1.call-start = ((), (), s32[]{:S(2)}) async-start(), calls=%async_computation.4 | async-start | bytes 2097152 | tf_op jit(solution)/shard_map/psum | solution.py:34
  249.6 3.5 %copy-start.1 = (bf16[2048,704]{0,1:T(8,128)(2,1)S(1)}, bf16[2048,704]{0,1:T(8,128)(2,1)}, u32[]{:S(2)}) copy-start(bf16[2048,704]{0,1:T(8,128)(2,1)} %all-gather.7.cloned.1.call-done) | copy-start | bytes 8650756
  249.6 3.5 %copy-start.5 = (f32[256,704]{0,1:T(8,128)S(1)}, f32[256,704]{0,1:T(8,128)}, u32[]{:S(2)}) copy-start(f32[256,704]{0,1:T(8,128)} %fusion.7) | copy-start | bytes 2162692
Sparse Core Ops, SparseCore 0:
  9.6 61.8 all-gather.8
  73.0 57.7 all-gather.6
  132.4 77.6 all-gather.4
  211.6 34.6 all-gather.10
  249.6 31.1 all-reduce.4
  283.6 36.2 all-reduce.2
where the time goes:
time: 329 us
  waiting for transfers between devices  221 us (67%)
  blocking collectives  68.9 us (21%)
  matrix products  19.2 us (6%)
  between operations  14.2 us (4%)
  local copies, waits for them, and re-layouts  3.4 us (1%)
    all_gather x1, waiting for transfers between devices, on_device(): lax.all_gather(gate_weight, 'fs', axis=0, tiled=True)  62 us
    all_to_all x1, blocking collectives, on_device(): lax.all_to_all(out_grad, 'fs', split_axis=1, concat_axis=0, tiled=True)  56.6 us
    all_gather x1, waiting for transfers between devices, on_device(): lax.all_gather(up_weight, 'fs', axis=0, tiled=True)  56.6 us
    all_gather x1, waiting for transfers between devices, on_device(): lax.all_gather(hidden, 'fs', axis=0, tiled=True)  32.2 us
    psum x1, waiting for transfers between devices, on_device(): shard = lax.psum(shard.astype(jnp.bfloat16), 'rep').astype(jnp.float32)  25.6 us
    psum x1, waiting for transfers between devices, on_device(): input_grad = lax.psum(partial_value.astype(jnp.bfloat16), 'tp')  24.5 us
    all_gather x1, waiting for transfers between devices, on_device(): down_full = lax.all_gather(down_weight, 'fs', axis=1, tiled=True)  17.8 us
    psum x1, blocking collectives, on_device(): norms = lax.psum(jnp.sum(shard * shard, axis=1), 'fs')  12.2 us
  transfers between devices with their start and end apart: 6, of which 6 were waited for; matrix products, arithmetic and copies ran while one was open for 6% of the time, Pallas kernels for 0%

commit v1 on v0

--- a/solution.py
+++ b/solution.py
@@ -32,7 +32,15 @@
     gate_grad = (hid_grad * up_pre * sigma * (1.0 + gate_pre * (1.0 - sigma))).astype(jnp.bfloat16)
     partial_value = contract_last(gate_grad, gate_full) + contract_last(up_grad, up_full)
     input_grad = lax.psum(partial_value.astype(jnp.bfloat16), "tp")
-    columns = lax.all_to_all(out_grad, "fs", split_axis=1, concat_axis=0, tiled=True)
+    columns = jnp.concatenate(
+        lax.all_to_all(
+            jnp.stack(jnp.split(out_grad, lax.axis_size("fs"), axis=1)),
+            "fs",
+            split_axis=0,
+            concat_axis=0,
+        ),
+        axis=0,
+    )
     shard = contract_first(lax.all_gather(hidden, "fs", axis=0, tiled=True), columns)
     shard = lax.psum(shard.astype(jnp.bfloat16), "rep").astype(jnp.float32)
     norms = lax.psum(jnp.sum(shard * shard, axis=1), "fs")

time: 329 us -> 331 us (level)
  blocking collectives: 68.9 us -> 12.2 us
  waiting for transfers between devices: 221 us -> 276 us
  starting transfers between devices: 0.24 us -> 3.77 us
    all_to_all x1 -> x0, blocking collectives: 56.6 us -> none  [on_device(): lax.all_to_all(out_grad, 'fs', split_axis=1, concat_axis=0, tiled=True)]
    all_gather x1, waiting for transfers between devices: 17.8 us -> 72.4 us  [on_device(): down_full = lax.all_gather(down_weight, 'fs', axis=1, tiled=True)]
    all_to_all x0 -> x1, starting transfers between devices: none -> 3.54 us  [on_device(): lax.all_to_all(jnp.stack(jnp.split(out_grad, lax.axis_size('fs'), axis=1)...]
  transfers between devices with their start and end apart: 6 -> 7, of which waited for: 6 -> 6; matrix products, arithmetic and copies ran while one was open for 6% -> 6% of each run, Pallas kernels for 0% -> 0%
where the time goes in v1:
time: 331 us
  waiting for transfers between devices  276 us (83%)
  matrix products  18.9 us (6%)
  between operations  14.2 us (4%)
  blocking collectives  12.2 us (4%)
  starting transfers between devices  3.77 us (1%)
  other arithmetic  3.45 us (1%)
    all_gather x1, waiting for transfers between devices, on_device(): down_full = lax.all_gather(down_weight, 'fs', axis=1, tiled=True)  72.4 us
    all_gather x1, waiting for transfers between devices, on_device(): lax.all_gather(gate_weight, 'fs', axis=0, tiled=True)  62 us
    all_gather x1, waiting for transfers between devices, on_device(): lax.all_gather(up_weight, 'fs', axis=0, tiled=True)  56.6 us
    all_gather x1, waiting for transfers between devices, on_device(): lax.all_gather(hidden, 'fs', axis=0, tiled=True)  32.5 us
    psum x1, waiting for transfers between devices, on_device(): shard = lax.psum(shard.astype(jnp.bfloat16), 'rep').astype(jnp.float32)  25.6 us
    psum x1, waiting for transfers between devices, on_device(): input_grad = lax.psum(partial_value.astype(jnp.bfloat16), 'tp')  24.5 us
    psum x1, blocking collectives, on_device(): norms = lax.psum(jnp.sum(shard * shard, axis=1), 'fs')  12.2 us
    dot_general x3, matrix products, contract_last(): lax.dot_general(left, right, (((1,), (1,)), ((), ())), preferred_element_...  9.2 us
  transfers between devices with their start and end apart: 7, of which 6 were waited for; matrix products, arithmetic and copies ran while one was open for 6% of the time, Pallas kernels for 0%

profile of v1, /device:TPU:0, one launch (start us, length us, event | category | flops | bytes accessed | tf_op | source)
XLA Modules:
  0.0 330.8 jit_solution(15749701673615155505)
XLA Ops:
  7.2 0.0 copy-start
  7.2 0.0 all-gather.9.cloned.1.call-start
  7.2 0.7 all-gather.9.cloned.1.call-update
  7.9 0.0 all-gather.7.cloned.1.call-start
  8.0 0.7 all-gather.7.cloned.1.call-update
  8.7 0.0 all-gather.5.cloned.1.call-start
  8.7 0.7 all-gather.5.cloned.1.call-update
  9.4 0.0 all-gather.11.cloned.1.call-start
  9.4 62.0 %all-gather.9.cloned.1.call-done = bf16[2048,704]{0,1:T(8,128)(2,1)} async-done(((bf16[512,704]{0,1:T(8,128)(2,1)}), bf16[2048,704]{0,1:T(8,128)(2,1)}) %all-gather.9.cloned.1.call-update) | async-done | bytes 2883600 | tf_op jit(solution)/shard_map/all_gather | solution.py:22
  71.4 0.0 copy-done
  71.4 2.8 fusion.8
  74.2 0.0 copy-start.3
  74.2 0.0 copy-start.2
  74.2 56.6 %all-gather.7.cloned.1.call-done = bf16[2048,704]{0,1:T(8,128)(2,1)} async-done(((bf16[512,704]{0,1:T(8,128)(2,1)}), bf16[2048,704]{0,1:T(8,128)(2,1)}) %all-gather.7.cloned.1.call-update) | async-done | bytes 2883600 | tf_op jit(solution)/shard_map/all_gather | solution.py:23
  130.8 3.7 %multiply_convert_fusion = (bf16[256,704]{0,1:T(8,128)(2,1)}, f32[256,704]{0,1:T(8,128)}) fusion(f32[256,704]{0,1:T(8,128)S(1)} %fusion.8, bf16[256,2048]{1,0:T(8,128)(2,1)S(1)} %copy-done, bf16[2048,704]{0,1:T(8,128)(2,1)} %all-gather.7.cloned.1.call-done), kind=kOutput, calls=%fused_computation.5 | convolution fusion | flops 739278848 | bytes 5734400 | tf_op jit(solution)/shard_map/dot_general | solution.py:26
  134.6 0.0 copy-done.3
  134.6 0.0 all-gather.11.cloned.1.call-update
  134.6 0.0 copy-done.2
  134.6 0.1 slice_bitcast_fusion.3
  134.7 1.1 pad_maximum_fusion
  135.8 3.5 %all-to-all-start = ((bf16[4,256,512]{2,1,0:T(8,128)(2,1)}), bf16[4,256,512]{2,1,0:T(8,128)(2,1)S(1)}, u32[]{:S(2)}, u32[]{:S(2)}) async-start(bf16[4,256,512]{2,1,0:T(8,128)(2,1)} %pad_maximum_fusion), calls=%async_computation | async-start | bytes 2097152 | tf_op jit(solution)/shard_map/all_to_all | solution.py:36
  139.4 0.0 all-reduce.5.cloned.1.call-start
  139.4 72.4 %all-gather.5.cloned.1.call-done = bf16[704,2048]{1,0:T(8,128)(2,1)} async-done(((bf16[704,512]{1,0:T(8,128)(2,1)}), bf16[704,2048]{1,0:T(8,128)(2,1)}) %all-gather.5.cloned.1.call-update) | async-done | bytes 2883600 | tf_op jit(solution)/shard_map/all_gather | solution.py:20
  211.8 3.7 %fusion.7 = f32[256,704]{0,1:T(8,128)} fusion(bf16[256,2048]{1,0:T(8,128)(2,1)S(1)} %copy-done.2, bf16[704,2048]{1,0:T(8,128)(2,1)} %all-gather.5.cloned.1.call-done), kind=kOutput, calls=%fused_computation.18 | convolution fusion | flops 738197504 | bytes 4653056 | tf_op jit(solution)/shard_map/dot_general | solution.py:8
  215.5 0.0 all-to-all-done
  215.5 32.5 %all-gather.11.cloned.1.call-done = bf16[1024,704]{0,1:T(8,128)(2,1)} async-done(((bf16[256,704]{0,1:T(8,128)(2,1)}), bf16[1024,704]{0,1:T(8,128)(2,1)}) %all-gather.11.cloned.1.call-update) | async-done | bytes 1441808 | tf_op jit(solution)/shard_map/all_gather | solution.py:44
  248.0 0.0 copy-start.4
  248.0 3.2 convolution_convert_fusion
  251.2 0.0 all-reduce.5.cloned.1.call-update
  251.2 0.0 all-reduce.3.cloned.1.call-start
  251.3 0.0 copy-done.4
  251.3 0.0 copy-start.1
  251.3 0.0 copy-start.5
  251.3 3.5 %fusion.2 = f32[256,2048]{1,0:T(8,128)S(1)} fusion(bf16[2048,704]{0,1:T(8,128)(2,1)} %all-gather.9.cloned.1.call-done, f32[256,704]{0,1:T(8,128)S(1)} %copy-done.4, f32[256,704]{0,1:T(8,128)} %fusion.7, f32[256,704]{0,1:T(8,128)} %get-tuple-element.10), kind=kOutput, calls=%fused_computation.10 | convolution fusion | flops 739999744 | bytes 7143424 | tf_op jit(solution)/shard_map/dot_general | solution.py:8
  254.8 0.0 copy-done.1
  254.8 0.0 copy-done.5
  254.8 2.0 fusion
  256.9 0.0 all-reduce.3.cloned.1.call-update
  256.9 25.6 %all-reduce.5.cloned.1.call-done = bf16[704,512]{1,0:T(8,128)(2,1)} async-done(((bf16[704,512]{1,0:T(8,128)(2,1)}), bf16[704,512]{1,0:T(8,128)(2,1)}) %all-reduce.5.cloned.1.call-update) | async-done | bytes 720912 | tf_op jit(solution)/shard_map/psum | solution.py:45
  282.5 2.3 multiply_reduce_fusion
  284.9 12.2 %psum.23 = f32[704]{0:T(1024)} all-reduce(f32[704]{0:T(1024)S(1)} %get-tuple-element.3), channel_id=1, replica_groups=mesh['rep'=2,'fs'=4,'tp'=4] {'fs'}, use_global_device_ids=true, to_apply=%region_3.0 | all-reduce | flops 704 | bytes 5632 | tf_op jit(solution)/shard_map/psum | solution.py:46
  297.1 24.5 %all-reduce.3.cloned.1.call-done = bf16[256,2048]{1,0:T(8,128)(2,1)} async-done(((bf16[256,2048]{1,0:T(8,128)(2,1)}), bf16[256,2048]{1,0:T(8,128)(2,1)}) %all-reduce.3.cloned.1.call-update) | async-done | bytes 1048592 | tf_op jit(solution)/shard_map/psum | solution.py:34
  321.6 2.3 copy.10
Async XLA Ops:
  7.2 64.3 %copy-start = (bf16[256,2048]{1,0:T(8,128)(2,1)S(1)}, bf16[256,2048]{1,0:T(8,128)(2,1)}, u32[]{:S(2)}) copy-start(bf16[256,2048]{1,0:T(8,128)(2,1)} %param.5) | copy-start | bytes 3145732
  7.2 64.2 %all-gather.9.cloned.1.call-start = ((), (), s32[]{:S(2)}) async-start(), calls=%async_computation.3 | async-start | bytes 3604480 | tf_op jit(solution)/shard_map/all_gather | solution.py:22
  7.9 122.9 %all-gather.7.cloned.1.call-start = ((), (), s32[]{:S(2)}) async-start(), calls=%async_computation.2 | async-start | bytes 3604480 | tf_op jit(solution)/shard_map/all_gather | solution.py:23
  8.7 203.2 %all-gather.5.cloned.1.call-start = ((), (), s32[]{:S(2)}) async-start(), calls=%async_computation.1 | async-start | bytes 3604480 | tf_op jit(solution)/shard_map/all_gather | solution.py:20
  9.4 238.6 %all-gather.11.cloned.1.call-start = ((), (), s32[]{:S(2)}) async-start(), calls=%async_computation.5 | async-start | bytes 1802240 | tf_op jit(solution)/shard_map/all_gather | solution.py:44
  74.2 60.4 %copy-start.3 = (f32[256,704]{0,1:T(8,128)}, f32[256,704]{0,1:T(8,128)S(1)}, u32[]{:S(2)}) copy-start(f32[256,704]{0,1:T(8,128)S(1)} %fusion.8) | copy-start | bytes 2162692
  74.2 60.4 %copy-start.2 = (bf16[256,2048]{1,0:T(8,128)(2,1)S(1)}, bf16[256,2048]{1,0:T(8,128)(2,1)}, u32[]{:S(2)}) copy-start(bf16[256,2048]{1,0:T(8,128)(2,1)} %param.9) | copy-start | bytes 3145732
  135.8 79.7 %all-to-all-start = ((bf16[4,256,512]{2,1,0:T(8,128)(2,1)}), bf16[4,256,512]{2,1,0:T(8,128)(2,1)S(1)}, u32[]{:S(2)}, u32[]{:S(2)}) async-start(bf16[4,256,512]{2,1,0:T(8,128)(2,1)} %pad_maximum_fusion), calls=%async_computation | async-start | bytes 2097152 | tf_op jit(solution)/shard_map/all_to_all | solution.py:36
  139.4 143.2 %all-reduce.5.cloned.1.call-start = ((), (), s32[]{:S(2)}) async-start(), calls=%async_computation.6 | async-start | bytes 1441792 | tf_op jit(solution)/shard_map/psum | solution.py:45
  248.0 3.3 copy-start.4
  251.2 70.4 %all-reduce.3.cloned.1.call-start = ((), (), s32[]{:S(2)}) async-start(), calls=%async_computation.4 | async-start | bytes 2097152 | tf_op jit(solution)/shard_map/psum | solution.py:34
  251.3 3.5 %copy-start.1 = (bf16[2048,704]{0,1:T(8,128)(2,1)S(1)}, bf16[2048,704]{0,1:T(8,128)(2,1)}, u32[]{:S(2)}) copy-start(bf16[2048,704]{0,1:T(8,128)(2,1)} %all-gather.7.cloned.1.call-done) | copy-start | bytes 8650756
  251.3 3.5 %copy-start.5 = (f32[256,704]{0,1:T(8,128)S(1)}, f32[256,704]{0,1:T(8,128)}, u32[]{:S(2)}) copy-start(f32[256,704]{0,1:T(8,128)} %fusion.7) | copy-start | bytes 2162692
Sparse Core Ops, SparseCore 0:
  9.6 61.8 all-gather.8
  73.0 57.7 all-gather.6
  132.4 79.3 all-gather.4
  213.3 34.6 all-gather.10
  251.4 31.1 all-reduce.4
  285.3 36.2 all-reduce.2
